TPU v7x, 32 devices: a whole 2x2x4 slice. The times are simulated.
32 devices in a mesh: row: 8 (over z, x), col: 4 (over y, core).
Axes of the slice: x: 2, y: 2, z: 4, core: 2. Of those that a mesh axis runs over, the one named last changes fastest.
Arguments:
- tokens: bfloat16 [8192, 2048], P('row'), may hold values from -136 to 136
- norm_gain: float32 [2048], replicated, may hold values from 0.1 to 1.9
- w_in: bfloat16 [2048, 1024], P(None, 'col'), may hold values from -0.125 to 0.125
- w_out: bfloat16 [1024, 2048], P(None, 'col'), may hold values from -0.1875 to 0.1875
Outputs:
- mixed_tokens: bfloat16 [8192, 2048], P('row', 'col')
All inputs are finite; a program needn't handle non-finite values.
Results may differ from a plain program's by a relative error of at most 0.013.
Values may be sent and summed in bfloat16 or wider, within the bound.
A program may use at most 64 MiB of HBM per device.

v0:
```python
import functools
import math

import jax
import jax.numpy as jnp
import numpy as np
from jax import lax
from jax.experimental import pallas as pl
from jax.experimental.pallas import tpu as pltpu
from jax.sharding import PartitionSpec as P

GROUP = 256


NORM_EPS = 1e-06


def as_sent(array):

    def short(part):
        return part.astype(jnp.bfloat16) if part.dtype == jnp.float32 else part

    return jax.tree.map(short, array)


def rotation_table(first_index, second_index, spectral_magnitude, factor):
    phase = (first_index * second_index % spectral_magnitude).astype(jnp.float32) * (
        2.0 * math.pi / spectral_magnitude
    )
    return (jnp.cos(phase) * factor, jnp.sin(phase) * factor)


def twiddle(real_input_values, imag_in, freq_index, pos_index, spectral_magnitude):
    cosine, sine = rotation_table(freq_index, pos_index, spectral_magnitude, 1.0)
    return (
        real_input_values * cosine + imag_in * sine,
        imag_in * cosine - real_input_values * sine,
    )


def second_section(stacked, half):
    length_dev = stacked.shape[1]
    stride = min(length_dev, 512)
    positions = lax.broadcasted_iota(jnp.int32, (length_dev, stride), 0)
    real_blocks = []
    imag_blocks = []
    for offset in range(0, length_dev, stride):
        freqs = lax.broadcasted_iota(jnp.int32, (length_dev, stride), 1) + offset
        cosine, sine = rotation_table(positions, freqs, length_dev, 1.0)
        with_cos = jnp.dot(stacked, cosine, precision=lax.Precision.HIGH)
        with_sin = jnp.dot(stacked, sine, precision=lax.Precision.HIGH)
        real_blocks.append(with_cos[:half] + with_sin[half:])
        imag_blocks.append(with_cos[half:] - with_sin[:half])
    return (jnp.concatenate(real_blocks, 1), jnp.concatenate(imag_blocks, 1))


def reorder_positions(arrived):
    channels, row_count, _, block_len = arrived.shape
    return jnp.swapaxes(arrived.reshape(channels, row_count, block_len), 1, 2).reshape(
        channels, row_count * block_len
    )


def local(tokens, norm_gain, w_in, w_out):
    length_dev = tokens.shape[0]
    row_count = lax.axis_size("row")
    col_count = lax.axis_size("col")
    total_len = length_dev * row_count
    widened = tokens.astype(jnp.float32)
    inverse = lax.rsqrt(jnp.mean(widened * widened, axis=1, keepdims=True) + NORM_EPS)
    normed = (widened * inverse * norm_gain[None, :]).astype(jnp.bfloat16)
    projected = lax.dot_general(
        w_in, normed, (((0,), (1,)), ((), ())), preferred_element_type=jnp.float32
    ).astype(jnp.bfloat16)
    channels = projected.shape[0]
    block_len = length_dev // row_count
    small_cos, small_sin = rotation_table(
        lax.broadcasted_iota(jnp.int32, (row_count, row_count), 0),
        lax.broadcasted_iota(jnp.int32, (row_count, row_count), 1),
        row_count,
        1.0 / math.sqrt(total_len),
    )
    per_row = channels // row_count
    arrived = lax.all_to_all(
        projected.reshape(channels, 1, length_dev), "row", split_axis=0, concat_axis=1, tiled=True
    )
    values = arrived.astype(jnp.float32)
    real_one = jnp.einsum("ka,cab->ckb", small_cos, values, precision=lax.Precision.HIGH)
    imag_one = -jnp.einsum("ka,cab->ckb", small_sin, values, precision=lax.Precision.HIGH)
    freq_index = lax.broadcasted_iota(jnp.int32, (row_count, length_dev), 0)
    pos_index = lax.broadcasted_iota(jnp.int32, (row_count, length_dev), 1)
    real_two, imag_two = twiddle(real_one, imag_one, freq_index, pos_index, total_len)
    stacked = jnp.concatenate(
        [
            real_two.reshape(per_row * row_count, length_dev),
            imag_two.reshape(per_row * row_count, length_dev),
        ],
        0,
    )
    real_three, imag_three = second_section(stacked, per_row * row_count)
    shaped = (per_row, row_count, row_count, block_len)
    back_real, back_imag = (
        lax.all_to_all(
            real_three.reshape(shaped).astype(jnp.bfloat16),
            "row",
            split_axis=2,
            concat_axis=0,
            tiled=True,
        ).astype(jnp.float32),
        lax.all_to_all(
            imag_three.reshape(shaped).astype(jnp.bfloat16),
            "row",
            split_axis=2,
            concat_axis=0,
            tiled=True,
        ).astype(jnp.float32),
    )
    spec_real = reorder_positions(back_real)
    spec_imag = reorder_positions(back_imag)
    quarter = length_dev // col_count
    group_cosine_table, group_sine_table = rotation_table(
        lax.broadcasted_iota(jnp.int32, (GROUP, GROUP), 0),
        lax.broadcasted_iota(jnp.int32, (GROUP, GROUP), 1),
        GROUP,
        1.0 / math.sqrt(GROUP),
    )
    real_input_values = lax.all_to_all(
        as_sent(spec_real.reshape(channels, col_count, quarter)),
        "col",
        split_axis=1,
        concat_axis=0,
        tiled=True,
    )
    imag_in = lax.all_to_all(
        as_sent(spec_imag.reshape(channels, col_count, quarter)),
        "col",
        split_axis=1,
        concat_axis=0,
        tiled=True,
    )
    width_all = real_input_values.shape[0]
    item_count = real_input_values.shape[2]
    groups = width_all // GROUP
    real_by_group = real_input_values.reshape(groups, GROUP, item_count)
    imaginary_by_group = imag_in.reshape(groups, GROUP, item_count)
    merged_spectrum = jnp.einsum(
        "hz,azo->aho", group_cosine_table, real_by_group, precision=lax.Precision.HIGH
    )
    merged_spectrum = merged_spectrum + jnp.einsum(
        "hz,azo->aho", group_sine_table, imaginary_by_group, precision=lax.Precision.HIGH
    )
    result = merged_spectrum.reshape(width_all, 1, item_count).astype(jnp.bfloat16)
    spectral = lax.all_to_all(result, "col", split_axis=0, concat_axis=1, tiled=True)
    output = lax.dot_general(
        lax.all_gather(spectral.reshape(channels, length_dev), "col", axis=0, tiled=True),
        w_out,
        (((0,), (0,)), ((), ())),
        preferred_element_type=jnp.float32,
    )
    return output.astype(jnp.bfloat16)


HALVES = 2
POINTS = 8
SPLIT = 1
LANES = 128
MESH = pl.DeviceIdType.MESH


def channel_tables(group, total_len):
    half = group // 2
    index = np.arange(group)
    angle = 2.0 * np.pi * (index[:, None] * index[None, :] % group) / group
    transform = np.concatenate([np.cos(angle[: half + 1]), np.sin(angle[1:half])], 0)
    fold = np.zeros((group, group))
    for k in range(half + 1):
        fold[k, k] = 1.0
        fold[k, -k % group] = 1.0
    for k in range(1, half):
        fold[half + k, group - k] = 1.0
        fold[half + k, k] = -1.0
    return (transform / math.sqrt(group)).astype(jnp.bfloat16), fold.astype(jnp.bfloat16)


def position_tables(block, total_len):
    j = np.arange(block)
    angle = 2.0 * np.pi * (np.arange(POINTS)[:, None] * j[None, :]) / total_len
    twiddles = np.stack([np.cos(angle), np.sin(angle)]).astype(np.float32)
    root = 32
    coarse = 2.0 * np.pi * (np.arange(block // root)[:, None] * root * j[None, :] % block) / block
    fine = 2.0 * np.pi * (np.arange(root)[:, None] * j[None, :] % block) / block
    scale = 1.0 / math.sqrt(total_len)
    coarse = np.stack([np.cos(coarse), np.sin(coarse)]).astype(np.float32)
    fine = np.stack([np.cos(fine) * scale, np.sin(fine) * scale]).astype(np.float32)
    return twiddles, coarse, fine


def eight_points(x):
    a = [x[i] + x[i + 4] for i in range(4)]
    b = [x[i] - x[i + 4] for i in range(4)]
    even, odd = a[0] + a[2], a[1] + a[3]
    root = math.sqrt(0.5)
    minus, plus = root * (b[1] - b[3]), root * (b[1] + b[3])
    one = (b[0] + minus, -b[2] - plus)
    two = (a[0] - a[2], a[3] - a[1])
    three = (b[0] - minus, b[2] - plus)
    return [
        (even + odd, None),
        one,
        two,
        three,
        (even - odd, None),
        (three[0], -three[1]),
        (two[0], -two[1]),
        (one[0], -one[1]),
    ]


def mixer_kernel(
    steps, ahead,
    tokens_hbm, gain_hbm, w_in_hbm, w_out_hbm, forward_hbm, fold_hbm, twiddle_hbm, coarse_hbm, fine_hbm,
    out_ref,
    tokens, gain, w_in, w_out, forward, fold, twiddles, coarse, fine,
    packed, arrived, stage, table, ready, gathered, folded, total,
    token_sem, load_sem, own_sem, send_one, recv_one, send_two, recv_two, send_col, recv_col,
):
    row, col = lax.axis_index("row"), lax.axis_index("col")
    rows = packed.shape[1]
    block, width = packed.shape[3], w_in.shape[1]
    size = block // steps
    part = packed.shape[2]
    flip = lambda index, bit: index + bit - 2 * bit * (index // bit % 2)
    sibling, across = flip(col, 1), flip(col, 2)

    def mate(d):
        index = row
        for bit in (1, 2, 4):
            if d & bit:
                index = flip(index, bit)
        return index

    loads = [
        pltpu.make_async_copy(src, dst, load_sem.at[i])
        for i, (src, dst) in enumerate([
            (w_in_hbm, w_in), (gain_hbm, gain), (forward_hbm, forward), (coarse_hbm, coarse), (fine_hbm, fine),
            (twiddle_hbm, twiddles), (fold_hbm, fold), (w_out_hbm, w_out),
        ])
    ]
    token_loads = [
        pltpu.make_async_copy(
            tokens_hbm.at[pl.ds(p * size, size)], tokens.at[pl.ds(p * size, size)], token_sem.at[p]
        )
        for p in range(steps)
    ]
    for load in loads[:3] + token_loads[:ahead]:
        load.start()

    barrier = pltpu.get_barrier_semaphore()
    peers = [(mate(d), col) for d in range(1, rows)] + [(row, sibling), (row, across)]
    for peer in peers:
        pl.semaphore_signal(barrier, inc=1, device_id=peer, device_id_type=MESH)

    def remote(src, dst, send, recv, device):
        return pltpu.make_async_remote_copy(
            src_ref=src, dst_ref=dst, send_sem=send, recv_sem=recv, device_id=device, device_id_type=MESH
        )

    def first_send(h, d, p=None):
        peer = mate(d)
        where = pl.ds(0, block) if p is None else pl.ds(p * size, size)
        return remote(
            packed.at[h, peer, :, where], arrived.at[h, row, :, where],
            send_one.at[h, d], recv_one.at[h, d], (peer, col),
        )

    order = [4, 5, 6, 7, 2, 3, 1]
    for load in loads[:3]:
        load.wait()
    for p in range(steps):
        token_loads[p].wait()
        if p + ahead < steps:
            token_loads[p + ahead].start()
        elif p + ahead == steps:
            for load in loads[3:]:
                load.start()
        where = slice(p * size, (p + 1) * size)
        wide = tokens[where, :].astype(jnp.float32)
        inverse = lax.rsqrt(jnp.mean(wide * wide, axis=1, keepdims=True) + NORM_EPS)
        normed = (wide * inverse * gain[...]).astype(jnp.bfloat16)
        projected = jnp.dot(normed, w_in[...], preferred_element_type=jnp.float32).astype(jnp.bfloat16)
        kept = lax.dot_general(
            forward[...], projected, (((1,), (1,)), ((), ())), preferred_element_type=jnp.float32
        )
        packed[:, :, :, where] = kept.astype(jnp.bfloat16).reshape(HALVES, rows, part, size)
        if p == 0:
            pl.semaphore_wait(barrier, len(peers))
        for d in order:
            first_send(0, d, p).start()
    for d in order:
        first_send(1, d).start()
    own_one = [
        pltpu.make_async_copy(packed.at[h, row], arrived.at[h, row], own_sem.at[h]) for h in range(HALVES)
    ]
    for copy in own_one:
        copy.start()
    for load in loads[3:]:
        load.wait()

    root = fine.shape[1]

    def table_rows(a, carry):
        cos_a, sin_a = coarse[0, pl.ds(a, 1), :], coarse[1, pl.ds(a, 1), :]
        at = pl.multiple_of(a * root, root)
        table[pl.ds(at, root), :] = (cos_a * fine[0] - sin_a * fine[1]).astype(jnp.bfloat16)
        table[pl.ds(block + at, root), :] = (sin_a * fine[0] + cos_a * fine[1]).astype(jnp.bfloat16)
        return carry

    lax.fori_loop(0, block // root, table_rows, 0)
    cols = w_out.shape[0] // width
    half = width // HALVES
    for c in range(cols):
        rows_out = jnp.dot(
            fold[...], w_out[c * width : (c + 1) * width, :], preferred_element_type=jnp.float32
        ).astype(jnp.bfloat16)
        for h in range(HALVES):
            folded[h, c * half : (c + 1) * half, :] = rows_out[h * half : (h + 1) * half]

    cut = POINTS // SPLIT

    def second_send(g, d):
        h, where = g // SPLIT, pl.ds(g % SPLIT * cut, cut)
        peer = mate(d)
        return remote(
            ready.at[h, peer, where], gathered.at[h, col, row, where],
            send_two.at[g, d], recv_two.at[g, d], (peer, col),
        )

    def keep(g):
        h, where = g // SPLIT, pl.ds(g % SPLIT * cut, cut)
        return pltpu.make_async_copy(
            ready.at[h, row, where], gathered.at[h, col, row, where], own_sem.at[HALVES + g]
        )

    span = 2 * LANES
    count = block // span
    other = (1 - row // (rows // 2)) * (count // 2)
    far, close = order[: rows // 2], order[rows // 2 :]
    for h in range(HALVES):
        own_one[h].wait()
        for d in order:
            first_send(h, d).wait_recv()

        def section(t, carry):
            at = pl.multiple_of(t * LANES, LANES)
            x = [arrived[h, r, :, pl.ds(at, LANES)].astype(jnp.float32) for r in range(rows)]
            points = eight_points(x)
            for k in range(POINTS):
                real, imag = points[k]
                if k > 0:
                    cosine = twiddles[0, k : k + 1, pl.ds(at, LANES)]
                    sine = twiddles[1, k : k + 1, pl.ds(at, LANES)]
                    if imag is None:
                        real, imag = real * cosine, -real * sine
                    else:
                        real, imag = real * cosine + imag * sine, imag * cosine - real * sine
                else:
                    imag = jnp.zeros_like(real)
                if h == 1:
                    place = lax.broadcasted_iota(jnp.int32, real.shape, 0) + row * part
                    plain = place == 0
                    real, imag = jnp.where(plain, real, -imag), jnp.where(plain, imag, real)
                stage[k, :, pl.ds(at, LANES)] = real.astype(jnp.bfloat16)
                stage[k, :, pl.ds(pl.multiple_of(block + at, LANES), LANES)] = imag.astype(jnp.bfloat16)
            return carry

        lax.fori_loop(0, block // LANES, section, 0)
        values = stage[...].reshape(POINTS * part, 2 * block)
        for i in range(count):
            n = lax.rem(other + i, count)
            done = jnp.dot(
                values, table[:, pl.ds(pl.multiple_of(n * span, span), span)], preferred_element_type=jnp.float32
            ).astype(jnp.bfloat16)
            for q in range(2):
                ready[h, 2 * n + q] = done[:, q * LANES : (q + 1) * LANES].reshape(POINTS, part, LANES)
            if i == count // 2 - 1:
                for g in range(h * SPLIT, (h + 1) * SPLIT):
                    for d in far:
                        second_send(g, d).start()
        for g in range(h * SPLIT, (h + 1) * SPLIT):
            for d in close:
                second_send(g, d).start()
            keep(g).start()

    def along(g, way, owner, target, d):
        spot = gathered.at[g // SPLIT, owner, mate(d), pl.ds(g % SPLIT * cut, cut)]
        return remote(spot, spot, send_col.at[g, way, d], recv_col.at[g, way, d], (row, target))

    def to_across(g, d):
        return along(g, 0, col, across, d)

    def to_sibling(g, d):
        return along(g, 1, col, sibling, d)

    def on_to_sibling(g, d):
        return along(g, 2, across, sibling, d)

    near, every = [0] + close[::-1], [0] + close[::-1] + far

    def relay(g, origins):
        for d in origins:
            if d == 0:
                keep(g).wait()
            else:
                second_send(g, d).wait_recv()
            to_across(g, d).start()
            to_sibling(g, d).start()

    def pass_on(g, origins):
        for d in origins:
            to_across(g, d).wait_recv()
            on_to_sibling(g, d).start()

    def collect(g):
        for d in every:
            to_sibling(g, d).wait_recv()
            on_to_sibling(g, d).wait_recv()

    def map_out(h, k):
        spectrum = gathered[h, :, :, k].reshape(cols * rows * part, LANES)
        piece = lax.dot_general(
            spectrum, folded[h], (((0,), (0,)), ((), ())), preferred_element_type=jnp.float32
        )
        total[k] = piece if h == 0 else total[k] + piece

    def map_part(g):
        for k in range(g % SPLIT * cut, (g % SPLIT + 1) * cut):
            map_out(g // SPLIT, k)

    relay(0, every)
    for d in every:
        relay(1, [d])
        pass_on(0, [d])
    collect(0)
    for k, d in enumerate(every):
        map_out(0, k)
        pass_on(1, [d])
    collect(1)
    map_part(1)
    out_ref[...] = jnp.swapaxes(total[...], 0, 1).reshape(out_ref.shape).astype(out_ref.dtype)

    for h in range(HALVES):
        for d in order:
            first_send(h, d).wait_send()
    for g in range(HALVES * SPLIT):
        for d in order:
            second_send(g, d).wait_send()
        for d in every:
            to_across(g, d).wait_send()
            to_sibling(g, d).wait_send()
            on_to_sibling(g, d).wait_send()


def fused(tokens, norm_gain, w_in, w_out):
    rows, cols = lax.axis_size("row"), lax.axis_size("col")
    block, width_in = tokens.shape
    width = w_in.shape[1]
    features = w_out.shape[1]
    part = width // (HALVES * rows)
    steps = 4
    forward, fold = channel_tables(width, block * rows)
    twiddles, coarse, fine = position_tables(block, block * rows)
    half, short, wide = jnp.bfloat16, pltpu.VMEM, jnp.float32
    operands = [tokens, norm_gain[None, :], w_in, w_out, forward, fold, twiddles, coarse, fine]
    operands = [jnp.asarray(x) for x in operands]
    dma = pltpu.SemaphoreType.DMA
    return pl.pallas_call(
        functools.partial(mixer_kernel, steps, 2),
        out_shape=jax.ShapeDtypeStruct((block, features), half),
        in_specs=[pl.BlockSpec(memory_space=pl.ANY)] * len(operands),
        out_specs=pl.BlockSpec(memory_space=pltpu.VMEM),
        scratch_shapes=[short(x.shape, x.dtype) for x in operands]
        + [
            short((HALVES, rows, part, block), half),
            short((HALVES, rows, part, block), half),
            short((POINTS, part, 2 * block), half),
            short((2 * block, block), half),
            short((HALVES, rows, POINTS, part, LANES), half),
            short((HALVES, cols, rows, POINTS, part, LANES), half),
            short((HALVES, w_out.shape[0] // HALVES, features), half),
            short((POINTS, LANES, features), wide),
            dma((steps,)),
            dma((8,)),
            dma((HALVES + HALVES * SPLIT,)),
            dma((HALVES, rows)),
            dma((HALVES, rows)),
            dma((HALVES * SPLIT, rows)),
            dma((HALVES * SPLIT, rows)),
            dma((HALVES * SPLIT, 3, rows)),
            dma((HALVES * SPLIT, 3, rows)),
        ],
        compiler_params=pltpu.CompilerParams(
            collective_id=0, has_side_effects=True, vmem_limit_bytes=60 * 1024 * 1024
        ),
    )(*operands)


def fits(mesh):
    return mesh.shape["row"] == POINTS and mesh.shape["col"] == 4


def choose(mesh, *arrays):
    tokens, _, w_in, _ = arrays
    group_local = w_in.shape[1] == GROUP
    tiles = tokens.shape[0] == POINTS * LANES
    return fused(*arrays) if fits(mesh) and group_local and tiles else local(*arrays)


def solution(mesh):
    placed = (P("row", None), P(), P(None, "col"), P(None, "col"))
    return jax.shard_map(
        functools.partial(choose, mesh), mesh=mesh, in_specs=placed, out_specs=P("row", "col"), check_vma=False
    )
```

profile of v0, /device:TPU:1, one launch (start us, length us, event | category | flops | bytes accessed | tf_op | source)
XLA Modules:
  0.0 42.9 jit_solution(4133393007618009898)
XLA Ops:
  0.0 40.6 %shard_map.91 = bf16[1024,512]{1,0:T(8,128)(2,1)} custom-call(bf16[1024,2048]{1,0:T(8,128)(2,1)} %tokens_hbm.1, f32[1,2048]{1,0:T(1,128)} %bitcast.1, bf16[2048,256]{1,0:T(8,128)(2,1)} %w_in_hbm.1, bf16[1024,512]{1,0:T(8,128)(2,1)} %w_out_hbm.1, bf16[256,256]{1,0:T(8,128)(2,1)} %constant.10.clone.forward_hbm, bf16[256,256]{1,0:T(8,128)(2,1)} %constant.11.clone.fold_hbm, ...), custom_call_target="tpu_custom_call" | custom-call | tf_op jit(solution)/shard_map/pallas_call | solution.py:476
  40.6 2.3 %copy.11 = bf16[1024,512]{1,0:T(8,128)(2,1)} copy(bf16[1024,512]{1,0:T(8,128)(2,1)} %shard_map.91) | data formatting | bytes 2097152
where the time goes:
time: 43 us; the launch traced here: 42.9 us
  Pallas kernels  40.6 us (94%)
  local copies, waits for them, and re-layouts  2.26 us (5%)
    pallas_call x1, Pallas kernels, fused(): pl.pallas_call(functools.partial(mixer_kernel, steps, 2), out_shape=jax.S...  40.6 us
    unnamed x1, local copies, waits for them, and re-layouts  2.26 us

commit v1 on v0

--- a/solution.py
+++ b/solution.py
@@ -471,7 +471,7 @@
     twiddles, coarse, fine = position_tables(block, block * rows)
     half, short, wide = jnp.bfloat16, pltpu.VMEM, jnp.float32
     operands = [tokens, norm_gain[None, :], w_in, w_out, forward, fold, twiddles, coarse, fine]
-    operands = [jnp.asarray(x) for x in operands]
+    operands = [pltpu.with_memory_space_constraint(jnp.asarray(x), pltpu.HBM) for x in operands]
     dma = pltpu.SemaphoreType.DMA
     return pl.pallas_call(
         functools.partial(mixer_kernel, steps, 2),
@@ -499,7 +499,7 @@
             dma((HALVES * SPLIT, 3, rows)),
         ],
         compiler_params=pltpu.CompilerParams(
-            collective_id=0, has_side_effects=True, vmem_limit_bytes=60 * 1024 * 1024
+            collective_id=0, has_side_effects=True, vmem_limit_bytes=32 * 1024 * 1024
         ),
     )(*operands)
 

time: 43 us -> 40.8 us (0.949)
  local copies, waits for them, and re-layouts: 2.26 us -> 0.97 us
  Pallas kernels: 40.6 us -> 39.6 us
    unnamed x1, local copies, waits for them, and re-layouts: 2.26 us -> 0.97 us
    pallas_call x1, Pallas kernels: 40.6 us -> 39.6 us  [fused(): pl.pallas_call(functools.partial(mixer_kernel, steps, 2), out_shape=jax.S...]
where the time goes in v1:
time: 40.8 us; the launch traced here: 40.6 us
  Pallas kernels  39.6 us (97%)
  local copies, waits for them, and re-layouts  0.97 us (2%)
    pallas_call x1, Pallas kernels, fused(): pl.pallas_call(functools.partial(mixer_kernel, steps, 2), out_shape=jax.S...  39.6 us
    unnamed x1, local copies, waits for them, and re-layouts  0.97 us

profile of v1, /device:TPU:1, one launch (start us, length us, event | category | flops | bytes accessed | tf_op | source)
XLA Modules:
  0.0 40.6 jit_solution(11873437640384569603)
XLA Ops:
  0.0 39.6 %shard_map.91 = bf16[1024,512]{1,0:T(8,128)(2,1)S(1)} custom-call(bf16[1024,2048]{1,0:T(8,128)(2,1)} %tokens_hbm.1, f32[1,2048]{1,0:T(1,128)} %bitcast.1, bf16[2048,256]{1,0:T(8,128)(2,1)} %w_in_hbm.1, bf16[1024,512]{1,0:T(8,128)(2,1)} %w_out_hbm.1, bf16[256,256]{1,0:T(8,128)(2,1)} %constant.10.clone.forward_hbm, bf16[256,256]{1,0:T(8,128)(2,1)} %constant.11.clone.fold_hbm, ...), custom_call_target="tpu_custom_call" | custom-call | tf_op jit(solution)/shard_map/pallas_call | solution.py:476
  39.6 1.0 %copy.11 = bf16[1024,512]{1,0:T(8,128)(2,1)} copy(bf16[1024,512]{1,0:T(8,128)(2,1)S(1)} %shard_map.91) | data formatting | bytes 2097152

commit v2 on v1

--- a/solution.py
+++ b/solution.py
@@ -162,7 +162,6 @@
 
 HALVES = 2
 POINTS = 8
-SPLIT = 1
 LANES = 128
 MESH = pl.DeviceIdType.MESH
 
@@ -217,12 +216,12 @@
 
 
 def mixer_kernel(
-    steps, ahead,
+    steps, ahead, direct,
     tokens_hbm, gain_hbm, w_in_hbm, w_out_hbm, forward_hbm, fold_hbm, twiddle_hbm, coarse_hbm, fine_hbm,
     out_ref,
     tokens, gain, w_in, w_out, forward, fold, twiddles, coarse, fine,
     packed, arrived, stage, table, ready, gathered, folded, total,
-    token_sem, load_sem, own_sem, send_one, recv_one, send_two, recv_two, send_col, recv_col,
+    token_sem, load_sem, send_one, recv_one, send_two, recv_near, recv_far, recv_direct, recv_relay, recv_share,
 ):
     row, col = lax.axis_index("row"), lax.axis_index("col")
     rows = packed.shape[1]
@@ -231,6 +230,8 @@
     part = packed.shape[2]
     flip = lambda index, bit: index + bit - 2 * bit * (index // bit % 2)
     sibling, across = flip(col, 1), flip(col, 2)
+    quarter = rows // 2
+    near, far = list(range(quarter)), list(range(quarter, rows))
 
     def mate(d):
         index = row
@@ -256,7 +257,8 @@
         load.start()
 
     barrier = pltpu.get_barrier_semaphore()
-    peers = [(mate(d), col) for d in range(1, rows)] + [(row, sibling), (row, across)]
+    peers = [(mate(d), col) for d in range(1, rows)] + [(row, sibling)]
+    peers += [(mate(d), across) for d in range(rows) if d == 0 or d in direct]
     for peer in peers:
         pl.semaphore_signal(barrier, inc=1, device_id=peer, device_id_type=MESH)
 
@@ -265,15 +267,13 @@
             src_ref=src, dst_ref=dst, send_sem=send, recv_sem=recv, device_id=device, device_id_type=MESH
         )
 
-    def first_send(h, d, p=None):
+    def first_send(h, d, where):
         peer = mate(d)
-        where = pl.ds(0, block) if p is None else pl.ds(p * size, size)
         return remote(
-            packed.at[h, peer, :, where], arrived.at[h, row, :, where],
-            send_one.at[h, d], recv_one.at[h, d], (peer, col),
-        )
-
-    order = [4, 5, 6, 7, 2, 3, 1]
+            packed.at[h, peer, :, where], arrived.at[h, row, :, where], send_one, recv_one.at[h], (peer, col)
+        )
+
+    order = far + [2, 3, 1]
     for load in loads[:3]:
         load.wait()
     for p in range(steps):
@@ -295,14 +295,11 @@
         if p == 0:
             pl.semaphore_wait(barrier, len(peers))
         for d in order:
-            first_send(0, d, p).start()
+            first_send(0, d, pl.ds(p * size, size)).start()
     for d in order:
-        first_send(1, d).start()
-    own_one = [
-        pltpu.make_async_copy(packed.at[h, row], arrived.at[h, row], own_sem.at[h]) for h in range(HALVES)
-    ]
-    for copy in own_one:
-        copy.start()
+        first_send(1, d, pl.ds(0, block)).start()
+    for h in range(HALVES):
+        arrived[h, row] = packed[h, row]
     for load in loads[3:]:
         load.wait()
 
@@ -323,32 +320,43 @@
             fold[...], w_out[c * width : (c + 1) * width, :], preferred_element_type=jnp.float32
         ).astype(jnp.bfloat16)
         for h in range(HALVES):
-            folded[h, c * half : (c + 1) * half, :] = rows_out[h * half : (h + 1) * half]
-
-    cut = POINTS // SPLIT
-
-    def second_send(g, d):
-        h, where = g // SPLIT, pl.ds(g % SPLIT * cut, cut)
+            folded[h, c] = rows_out[h * half : (h + 1) * half].reshape(rows, part, -1)
+
+    pieces = gathered.at[0, 0]
+    send_far, send_near, send_direct, send_relay, send_share = (send_two.at[i] for i in range(5))
+
+    def second_send(h, d):
+        peer = mate(d)
+        recv = recv_far.at[h, d - quarter] if d in far else recv_near.at[h]
+        return remote(
+            ready.at[h, peer], gathered.at[h, col, row], send_far if d in far else send_near, recv, (peer, col)
+        )
+
+    def direct_send(h, d):
         peer = mate(d)
         return remote(
-            ready.at[h, peer, where], gathered.at[h, col, row, where],
-            send_two.at[g, d], recv_two.at[g, d], (peer, col),
-        )
-
-    def keep(g):
-        h, where = g // SPLIT, pl.ds(g % SPLIT * cut, cut)
-        return pltpu.make_async_copy(
-            ready.at[h, row, where], gathered.at[h, col, row, where], own_sem.at[HALVES + g]
-        )
+            ready.at[h, peer], gathered.at[h, col, row], send_direct, recv_direct.at[h], (peer, across)
+        )
+
+    def relay_send(h, d):
+        spot = gathered.at[h, col, mate(d)]
+        recv = recv_relay.at[h, d // 2]
+        return remote(spot, spot, send_relay, recv, (row, across))
+
+    def share(h, owner, start, count, kind):
+        spot = gathered.at[h, owner, pl.ds(start, count)]
+        return remote(spot, spot, send_share, recv_share.at[h, kind], (row, sibling))
+
+    def waiter(count, send, recv):
+        group = pieces.at[pl.ds(0, count)]
+        return remote(group, group, send, recv, (row, sibling))
 
     span = 2 * LANES
-    count = block // span
-    other = (1 - row // (rows // 2)) * (count // 2)
-    far, close = order[: rows // 2], order[rows // 2 :]
     for h in range(HALVES):
-        own_one[h].wait()
-        for d in order:
-            first_send(h, d).wait_recv()
+        others = pl.ds(0, rows - 1)
+        remote(
+            packed.at[h, others], arrived.at[h, others], send_one, recv_one.at[h], (row, sibling)
+        ).wait_recv()
 
         def section(t, carry):
             at = pl.multiple_of(t * LANES, LANES)
@@ -375,89 +383,88 @@
 
         lax.fori_loop(0, block // LANES, section, 0)
         values = stage[...].reshape(POINTS * part, 2 * block)
-        for i in range(count):
-            n = lax.rem(other + i, count)
+        for base in (4, 6, 2, 0):
+            n = mate(base) // 2
             done = jnp.dot(
                 values, table[:, pl.ds(pl.multiple_of(n * span, span), span)], preferred_element_type=jnp.float32
             ).astype(jnp.bfloat16)
             for q in range(2):
                 ready[h, 2 * n + q] = done[:, q * LANES : (q + 1) * LANES].reshape(POINTS, part, LANES)
-            if i == count // 2 - 1:
-                for g in range(h * SPLIT, (h + 1) * SPLIT):
-                    for d in far:
-                        second_send(g, d).start()
-        for g in range(h * SPLIT, (h + 1) * SPLIT):
-            for d in close:
-                second_send(g, d).start()
-            keep(g).start()
-
-    def along(g, way, owner, target, d):
-        spot = gathered.at[g // SPLIT, owner, mate(d), pl.ds(g % SPLIT * cut, cut)]
-        return remote(spot, spot, send_col.at[g, way, d], recv_col.at[g, way, d], (row, target))
-
-    def to_across(g, d):
-        return along(g, 0, col, across, d)
-
-    def to_sibling(g, d):
-        return along(g, 1, col, sibling, d)
-
-    def on_to_sibling(g, d):
-        return along(g, 2, across, sibling, d)
-
-    near, every = [0] + close[::-1], [0] + close[::-1] + far
-
-    def relay(g, origins):
-        for d in origins:
-            if d == 0:
-                keep(g).wait()
-            else:
-                second_send(g, d).wait_recv()
-            to_across(g, d).start()
-            to_sibling(g, d).start()
-
-    def pass_on(g, origins):
-        for d in origins:
-            to_across(g, d).wait_recv()
-            on_to_sibling(g, d).start()
-
-    def collect(g):
-        for d in every:
-            to_sibling(g, d).wait_recv()
-            on_to_sibling(g, d).wait_recv()
-
-    def map_out(h, k):
-        spectrum = gathered[h, :, :, k].reshape(cols * rows * part, LANES)
+            for d in (base, base + 1):
+                if d > 0:
+                    second_send(h, d).start()
+                if d in direct:
+                    direct_send(h, d).start()
+        gathered[h, col, row] = ready[h, row]
+
+    base_near = row // quarter * quarter
+    base_far = quarter - base_near
+    pairs = [quarter // 2 + i for i in range(quarter // 2)]
+    pair_row = lambda pair: mate(2 * pair) // 2 * 2
+
+    def relay(h, d):
+        second_send(h, d).wait_recv()
+        relay_send(h, d).start()
+        if d % 2 == 1:
+            share(h, col, pair_row(d // 2), 2, 1).start()
+
+    def pass_on(h, pair):
+        waiter(2, send_relay, recv_relay.at[h, pair]).wait_recv()
+        share(h, across, pair_row(pair), 2, 1).start()
+
+    def share_near(h):
+        waiter(quarter - 1, send_near, recv_near.at[h]).wait_recv()
+        share(h, col, base_near, quarter, 0).start()
+        waiter(quarter, send_direct, recv_direct.at[h]).wait_recv()
+        share(h, across, base_near, quarter, 0).start()
+
+    def collect(h, kind):
+        waiter(rows, send_share, recv_share.at[h, kind]).wait_recv()
+
+    depth = cols * quarter * part
+
+    def map_out(h, kind, k):
+        start = base_far if kind else base_near
+        spectrum = gathered[h, :, pl.ds(start, quarter), k].reshape(depth, LANES)
+        weights = folded[h, :, pl.ds(start, quarter)].reshape(depth, -1)
         piece = lax.dot_general(
-            spectrum, folded[h], (((0,), (0,)), ((), ())), preferred_element_type=jnp.float32
-        )
-        total[k] = piece if h == 0 else total[k] + piece
-
-    def map_part(g):
-        for k in range(g % SPLIT * cut, (g % SPLIT + 1) * cut):
-            map_out(g // SPLIT, k)
-
-    relay(0, every)
-    for d in every:
-        relay(1, [d])
-        pass_on(0, [d])
-    collect(0)
-    for k, d in enumerate(every):
-        map_out(0, k)
-        pass_on(1, [d])
-    collect(1)
-    map_part(1)
+            spectrum, weights, (((0,), (0,)), ((), ())), preferred_element_type=jnp.float32
+        )
+        total[k] = piece if h == 0 and kind == 0 else total[k] + piece
+
+    def map_part(h, kind):
+        for k in range(POINTS):
+            map_out(h, kind, k)
+
+    for d in far:
+        relay(0, d)
+    share_near(0)
+    relay(1, far[0])
+    collect(0, 0)
+    map_part(0, 0)
+    for pair in pairs:
+        pass_on(0, pair)
+    for d in far[1:]:
+        relay(1, d)
+    share_near(1)
+    collect(0, 1)
+    map_part(0, 1)
+    collect(1, 0)
+    map_part(1, 0)
+    for pair in pairs:
+        pass_on(1, pair)
+    collect(1, 1)
+    map_part(1, 1)
     out_ref[...] = jnp.swapaxes(total[...], 0, 1).reshape(out_ref.shape).astype(out_ref.dtype)
 
-    for h in range(HALVES):
-        for d in order:
-            first_send(h, d).wait_send()
-    for g in range(HALVES * SPLIT):
-        for d in order:
-            second_send(g, d).wait_send()
-        for d in every:
-            to_across(g, d).wait_send()
-            to_sibling(g, d).wait_send()
-            on_to_sibling(g, d).wait_send()
+    others = pl.ds(0, rows - 1)
+    remote(packed.at[:, others], arrived.at[:, others], send_one, recv_one.at[0], (row, sibling)).wait_send()
+    waiter(HALVES * len(far), send_far, recv_far.at[0, 0]).wait_send()
+    waiter(HALVES * (quarter - 1), send_near, recv_near.at[0]).wait_send()
+    waiter(HALVES * len(direct), send_direct, recv_direct.at[0]).wait_send()
+    waiter(HALVES * len(far), send_relay, recv_relay.at[0, 0]).wait_send()
+    everything = gathered.at[0]
+    remote(everything, everything, send_share, recv_share.at[0, 0], (row, sibling)).wait_send()
 
 
 def fused(tokens, norm_gain, w_in, w_out):
@@ -473,8 +480,9 @@
     operands = [tokens, norm_gain[None, :], w_in, w_out, forward, fold, twiddles, coarse, fine]
     operands = [pltpu.with_memory_space_constraint(jnp.asarray(x), pltpu.HBM) for x in operands]
     dma = pltpu.SemaphoreType.DMA
+    direct = (0, 1, 2, 3)
     return pl.pallas_call(
-        functools.partial(mixer_kernel, steps, 2),
+        functools.partial(mixer_kernel, steps, 2, direct),
         out_shape=jax.ShapeDtypeStruct((block, features), half),
         in_specs=[pl.BlockSpec(memory_space=pl.ANY)] * len(operands),
         out_specs=pl.BlockSpec(memory_space=pltpu.VMEM),
@@ -486,17 +494,18 @@
             short((2 * block, block), half),
             short((HALVES, rows, POINTS, part, LANES), half),
             short((HALVES, cols, rows, POINTS, part, LANES), half),
-            short((HALVES, w_out.shape[0] // HALVES, features), half),
+            short((HALVES, cols, rows, part, features), half),
             short((POINTS, LANES, features), wide),
             dma((steps,)),
             dma((8,)),
-            dma((HALVES + HALVES * SPLIT,)),
-            dma((HALVES, rows)),
-            dma((HALVES, rows)),
-            dma((HALVES * SPLIT, rows)),
-            dma((HALVES * SPLIT, rows)),
-            dma((HALVES * SPLIT, 3, rows)),
-            dma((HALVES * SPLIT, 3, rows)),
+            dma(()),
+            dma((HALVES,)),
+            dma((5,)),
+            dma((HALVES,)),
+            dma((HALVES, rows // 2)),
+            dma((HALVES,)),
+            dma((HALVES, rows // 2)),
+            dma((HALVES, 2)),
         ],
         compiler_params=pltpu.CompilerParams(
             collective_id=0, has_side_effects=True, vmem_limit_bytes=32 * 1024 * 1024

time: 40.8 us -> 37.9 us (0.929)
  the two profiles are of different devices: /device:TPU:1 before, /device:TPU:9 now
where the time goes in v2:
time: 37.9 us; the launch traced here: 37.8 us
  Pallas kernels  36.8 us (97%)
  local copies, waits for them, and re-layouts  0.97 us (3%)
    pallas_call x1, Pallas kernels, fused(): pl.pallas_call(functools.partial(mixer_kernel, steps, 2, direct), out_sha...  36.8 us
    unnamed x1, local copies, waits for them, and re-layouts  0.97 us

profile of v2, /device:TPU:9, one launch (start us, length us, event | category | flops | bytes accessed | tf_op | source)
XLA Modules:
  0.0 37.8 jit_solution(16845113753021102188)
XLA Ops:
  0.0 36.8 %shard_map.91 = bf16[1024,512]{1,0:T(8,128)(2,1)S(1)} custom-call(bf16[1024,2048]{1,0:T(8,128)(2,1)} %tokens_hbm.1, f32[1,2048]{1,0:T(1,128)} %bitcast.1, bf16[2048,256]{1,0:T(8,128)(2,1)} %w_in_hbm.1, bf16[1024,512]{1,0:T(8,128)(2,1)} %w_out_hbm.1, bf16[256,256]{1,0:T(8,128)(2,1)} %constant.10.clone.forward_hbm, bf16[256,256]{1,0:T(8,128)(2,1)} %constant.11.clone.fold_hbm, ...), custom_call_target="tpu_custom_call" | custom-call | tf_op jit(solution)/shard_map/pallas_call | solution.py:484
  36.8 1.0 %copy.11 = bf16[1024,512]{1,0:T(8,128)(2,1)} copy(bf16[1024,512]{1,0:T(8,128)(2,1)S(1)} %shard_map.91) | data formatting | bytes 2097152

commit v3 on v2

--- a/solution.py
+++ b/solution.py
@@ -216,17 +216,19 @@
 
 
 def mixer_kernel(
-    steps, ahead, direct,
+    marks, ahead, groups,
     tokens_hbm, gain_hbm, w_in_hbm, w_out_hbm, forward_hbm, fold_hbm, twiddle_hbm, coarse_hbm, fine_hbm,
     out_ref,
     tokens, gain, w_in, w_out, forward, fold, twiddles, coarse, fine,
-    packed, arrived, stage, table, ready, gathered, folded, total,
+    packed, arrived, stage, table, ready, gathered, folded, total, spread,
     token_sem, load_sem, send_one, recv_one, send_two, recv_near, recv_far, recv_direct, recv_relay, recv_share,
 ):
     row, col = lax.axis_index("row"), lax.axis_index("col")
     rows = packed.shape[1]
     block, width = packed.shape[3], w_in.shape[1]
-    size = block // steps
+    edges = [block // LANES * LANES * i // 8 for i in marks]
+    chunks = [pl.ds(a, b - a) for a, b in zip(edges, edges[1:])]
+    steps = len(chunks)
     part = packed.shape[2]
     flip = lambda index, bit: index + bit - 2 * bit * (index // bit % 2)
     sibling, across = flip(col, 1), flip(col, 2)
@@ -248,17 +250,15 @@
         ])
     ]
     token_loads = [
-        pltpu.make_async_copy(
-            tokens_hbm.at[pl.ds(p * size, size)], tokens.at[pl.ds(p * size, size)], token_sem.at[p]
-        )
-        for p in range(steps)
+        pltpu.make_async_copy(tokens_hbm.at[where], tokens.at[where], token_sem.at[p])
+        for p, where in enumerate(chunks)
     ]
-    for load in loads[:3] + token_loads[:ahead]:
+    for load in [loads[1], loads[0], token_loads[0], loads[2]] + token_loads[1:ahead]:
         load.start()
 
     barrier = pltpu.get_barrier_semaphore()
     peers = [(mate(d), col) for d in range(1, rows)] + [(row, sibling)]
-    peers += [(mate(d), across) for d in range(rows) if d == 0 or d in direct]
+    peers += [(mate(d), across) for d in near]
     for peer in peers:
         pl.semaphore_signal(barrier, inc=1, device_id=peer, device_id_type=MESH)
 
@@ -274,30 +274,44 @@
         )
 
     order = far + [2, 3, 1]
-    for load in loads[:3]:
-        load.wait()
-    for p in range(steps):
+    edge = row // 2 % 3 == 0
+    loads[1].wait()
+    across_lanes = [
+        jnp.transpose(jnp.broadcast_to(gain[:, i : i + LANES], (LANES, LANES)))
+        for i in range(0, gain.shape[1], LANES)
+    ]
+    for i, scale in enumerate(across_lanes):
+        spread[i * LANES : (i + 1) * LANES, :] = scale
+    loads[0].wait()
+    for i in range(0, width, LANES):
+        lanes = slice(i, i + LANES)
+        w_in[:, lanes] = (w_in[:, lanes].astype(jnp.float32) * spread[...]).astype(jnp.bfloat16)
+    loads[2].wait()
+    for p, where in enumerate(chunks):
         token_loads[p].wait()
         if p + ahead < steps:
             token_loads[p + ahead].start()
         elif p + ahead == steps:
             for load in loads[3:]:
                 load.start()
-        where = slice(p * size, (p + 1) * size)
-        wide = tokens[where, :].astype(jnp.float32)
+        piece = tokens[where, :]
+        wide = piece.astype(jnp.float32)
         inverse = lax.rsqrt(jnp.mean(wide * wide, axis=1, keepdims=True) + NORM_EPS)
-        normed = (wide * inverse * gain[...]).astype(jnp.bfloat16)
-        projected = jnp.dot(normed, w_in[...], preferred_element_type=jnp.float32).astype(jnp.bfloat16)
+        projected = jnp.dot(piece, w_in[...], preferred_element_type=jnp.float32)
+        projected = (projected * inverse).astype(jnp.bfloat16)
         kept = lax.dot_general(
             forward[...], projected, (((1,), (1,)), ((), ())), preferred_element_type=jnp.float32
         )
-        packed[:, :, :, where] = kept.astype(jnp.bfloat16).reshape(HALVES, rows, part, size)
+        packed[:, :, :, where] = kept.astype(jnp.bfloat16).reshape(HALVES, rows, part, where.size)
         if p == 0:
             pl.semaphore_wait(barrier, len(peers))
         for d in order:
-            first_send(0, d, pl.ds(p * size, size)).start()
-    for d in order:
-        first_send(1, d, pl.ds(0, block)).start()
+            first_send(0, d, where).start()
+    def second_half():
+        for d in order:
+            first_send(1, d, pl.ds(0, block)).start()
+
+    second_half()
     for h in range(HALVES):
         arrived[h, row] = packed[h, row]
     for load in loads[3:]:
@@ -322,34 +336,57 @@
         for h in range(HALVES):
             folded[h, c] = rows_out[h * half : (h + 1) * half].reshape(rows, part, -1)
 
+    base_near = row // quarter * quarter
+    base_far = quarter - base_near
+    outer = base_far // quarter
     pieces = gathered.at[0, 0]
     send_far, send_near, send_direct, send_relay, send_share = (send_two.at[i] for i in range(5))
 
-    def second_send(h, d):
-        peer = mate(d)
-        recv = recv_far.at[h, d - quarter] if d in far else recv_near.at[h]
+    def near_send(h, d):
+        return remote(ready.at[h, mate(d)], gathered.at[h, col, row], send_near, recv_near.at[h], (mate(d), col))
+
+    def direct_send(h, d):
         return remote(
-            ready.at[h, peer], gathered.at[h, col, row], send_far if d in far else send_near, recv, (peer, col)
+            ready.at[h, mate(d)], gathered.at[h, col, row], send_direct, recv_direct.at[h], (mate(d), across)
         )
 
-    def direct_send(h, d):
-        peer = mate(d)
+    def spot(g, owner, place):
+        h, first, count = groups[g]
+        return gathered.at[h, owner, place, pl.ds(first, count)]
+
+    def crossing(level, f):
+        return base_far + 2 * level + flip(row % 2, f)
+
+    def far_send(g, level, f):
+        h, first, count = groups[g]
+        peer = crossing(level, f)
         return remote(
-            ready.at[h, peer], gathered.at[h, col, row], send_direct, recv_direct.at[h], (peer, across)
+            ready.at[h, peer, pl.ds(first, count)], spot(g, col, row),
+            send_far, recv_far.at[g, row % quarter], (peer, col),
         )
 
-    def relay_send(h, d):
-        spot = gathered.at[h, col, mate(d)]
-        recv = recv_relay.at[h, d // 2]
-        return remote(spot, spot, send_relay, recv, (row, across))
-
-    def share(h, owner, start, count, kind):
-        spot = gathered.at[h, owner, pl.ds(start, count)]
-        return remote(spot, spot, send_share, recv_share.at[h, kind], (row, sibling))
+    def far_arrival(g, level, f):
+        source = crossing(level, f)
+        place = spot(g, col, source)
+        return remote(place, place, send_far, recv_far.at[g, source % quarter], (source, col))
+
+    def relay_send(g, level, f):
+        place = spot(g, col, crossing(level, f))
+        return remote(place, place, send_relay, recv_relay.at[g], (row, across))
+
+    def share(place, kind):
+        return remote(place, place, send_share, recv_share.at[kind], (row, sibling))
 
     def waiter(count, send, recv):
         group = pieces.at[pl.ds(0, count)]
         return remote(group, group, send, recv, (row, sibling))
+
+    def cross(h):
+        for level in range(2):
+            for g in range(len(groups)):
+                for f in range(2):
+                    if groups[g][0] == h:
+                        far_send(g, level, f).start()
 
     span = 2 * LANES
     for h in range(HALVES):
@@ -383,88 +420,104 @@
 
         lax.fori_loop(0, block // LANES, section, 0)
         values = stage[...].reshape(POINTS * part, 2 * block)
-        for base in (4, 6, 2, 0):
-            n = mate(base) // 2
+        def columns(n):
             done = jnp.dot(
                 values, table[:, pl.ds(pl.multiple_of(n * span, span), span)], preferred_element_type=jnp.float32
             ).astype(jnp.bfloat16)
             for q in range(2):
                 ready[h, 2 * n + q] = done[:, q * LANES : (q + 1) * LANES].reshape(POINTS, part, LANES)
-            for d in (base, base + 1):
-                if d > 0:
-                    second_send(h, d).start()
-                if d in direct:
+
+        def nearby():
+            for step in range(2):
+                columns(mate(2 * step) // 2)
+                for d in (2 * step, 2 * step + 1):
+                    if d > 0:
+                        near_send(h, d).start()
                     direct_send(h, d).start()
+
+
+        def beyond():
+            for level in range(2):
+                columns(base_far // 2 + level)
+            cross(h)
+
+        for stage_of in (nearby, beyond):
+            stage_of()
         gathered[h, col, row] = ready[h, row]
 
-    base_near = row // quarter * quarter
-    base_far = quarter - base_near
-    pairs = [quarter // 2 + i for i in range(quarter // 2)]
-    pair_row = lambda pair: mate(2 * pair) // 2 * 2
-
-    def relay(h, d):
-        second_send(h, d).wait_recv()
-        relay_send(h, d).start()
-        if d % 2 == 1:
-            share(h, col, pair_row(d // 2), 2, 1).start()
-
-    def pass_on(h, pair):
-        waiter(2, send_relay, recv_relay.at[h, pair]).wait_recv()
-        share(h, across, pair_row(pair), 2, 1).start()
+    half_rows = lambda start: pl.ds(start, quarter)
+
+    def relay(g, level):
+        for f in range(2):
+            far_arrival(g, level, f).wait_recv()
+            relay_send(g, level, f).start()
+
+    def share_far(g):
+        share(spot(g, col, half_rows(base_far)), HALVES + g).start()
+
+    def pass_on(g):
+        place = spot(g, across, half_rows(base_far))
+        remote(place, place, send_relay, recv_relay.at[g], (row, across)).wait_recv()
+        share(place, HALVES + g).start()
 
     def share_near(h):
         waiter(quarter - 1, send_near, recv_near.at[h]).wait_recv()
-        share(h, col, base_near, quarter, 0).start()
+        share(gathered.at[h, col, half_rows(base_near)], h).start()
         waiter(quarter, send_direct, recv_direct.at[h]).wait_recv()
-        share(h, across, base_near, quarter, 0).start()
-
-    def collect(h, kind):
-        waiter(rows, send_share, recv_share.at[h, kind]).wait_recv()
+        share(gathered.at[h, across, half_rows(base_near)], h).start()
 
     depth = cols * quarter * part
 
-    def map_out(h, kind, k):
-        start = base_far if kind else base_near
-        spectrum = gathered[h, :, pl.ds(start, quarter), k].reshape(depth, LANES)
-        weights = folded[h, :, pl.ds(start, quarter)].reshape(depth, -1)
-        piece = lax.dot_general(
-            spectrum, weights, (((0,), (0,)), ((), ())), preferred_element_type=jnp.float32
-        )
-        total[k] = piece if h == 0 and kind == 0 else total[k] + piece
-
-    def map_part(h, kind):
-        for k in range(POINTS):
-            map_out(h, kind, k)
-
-    for d in far:
-        relay(0, d)
+    def map_out(h, start, points, fresh):
+        weights = folded[h, :, half_rows(start)].reshape(depth, -1)
+        for k in points:
+            spectrum = gathered[h, :, half_rows(start), k].reshape(depth, LANES)
+            piece = lax.dot_general(
+                spectrum, weights, (((0,), (0,)), ((), ())), preferred_element_type=jnp.float32
+            )
+            total[k] = piece if fresh else total[k] + piece
+
+    def map_near(h):
+        waiter(rows, send_share, recv_share.at[h]).wait_recv()
+        map_out(h, base_near, range(POINTS), h == 0)
+
+    def map_far(g):
+        h, first, count = groups[g]
+        both = gathered.at[h, pl.ds(0, 2), half_rows(base_far), pl.ds(first, count)]
+        remote(both, both, send_share, recv_share.at[HALVES + g], (row, sibling)).wait_recv()
+        map_out(h, base_far, range(first, first + count), False)
+
+    inner = 1 - outer
+    relay(0, outer)
+    relay(0, inner)
+    share_far(0)
     share_near(0)
-    relay(1, far[0])
-    collect(0, 0)
-    map_part(0, 0)
-    for pair in pairs:
-        pass_on(0, pair)
-    for d in far[1:]:
-        relay(1, d)
+    relay(1, outer)
+    relay(1, inner)
+    relay(2, outer)
+    relay(2, inner)
+    for g in range(1, len(groups)):
+        share_far(g)
+    pass_on(0)
+    map_near(0)
     share_near(1)
-    collect(0, 1)
-    map_part(0, 1)
-    collect(1, 0)
-    map_part(1, 0)
-    for pair in pairs:
-        pass_on(1, pair)
-    collect(1, 1)
-    map_part(1, 1)
+    map_far(0)
+    pass_on(1)
+    map_near(1)
+    for g in range(2, len(groups)):
+        pass_on(g)
+    for g in range(1, len(groups)):
+        map_far(g)
     out_ref[...] = jnp.swapaxes(total[...], 0, 1).reshape(out_ref.shape).astype(out_ref.dtype)
 
     others = pl.ds(0, rows - 1)
     remote(packed.at[:, others], arrived.at[:, others], send_one, recv_one.at[0], (row, sibling)).wait_send()
     waiter(HALVES * len(far), send_far, recv_far.at[0, 0]).wait_send()
     waiter(HALVES * (quarter - 1), send_near, recv_near.at[0]).wait_send()
-    waiter(HALVES * len(direct), send_direct, recv_direct.at[0]).wait_send()
-    waiter(HALVES * len(far), send_relay, recv_relay.at[0, 0]).wait_send()
+    waiter(HALVES * quarter, send_direct, recv_direct.at[0]).wait_send()
+    waiter(HALVES * len(far), send_relay, recv_relay.at[0]).wait_send()
     everything = gathered.at[0]
-    remote(everything, everything, send_share, recv_share.at[0, 0], (row, sibling)).wait_send()
+    remote(everything, everything, send_share, recv_share.at[0], (row, sibling)).wait_send()
 
 
 def fused(tokens, norm_gain, w_in, w_out):
@@ -473,16 +526,16 @@
     width = w_in.shape[1]
     features = w_out.shape[1]
     part = width // (HALVES * rows)
-    steps = 4
+    marks = (0, 1, 2, 3, 4, 5, 6, 7, 8)
     forward, fold = channel_tables(width, block * rows)
     twiddles, coarse, fine = position_tables(block, block * rows)
     half, short, wide = jnp.bfloat16, pltpu.VMEM, jnp.float32
     operands = [tokens, norm_gain[None, :], w_in, w_out, forward, fold, twiddles, coarse, fine]
     operands = [pltpu.with_memory_space_constraint(jnp.asarray(x), pltpu.HBM) for x in operands]
     dma = pltpu.SemaphoreType.DMA
-    direct = (0, 1, 2, 3)
+    groups = ((0, 0, POINTS), (1, 0, POINTS // 2), (1, POINTS // 2, POINTS // 2))
     return pl.pallas_call(
-        functools.partial(mixer_kernel, steps, 2, direct),
+        functools.partial(mixer_kernel, marks, 4, groups),
         out_shape=jax.ShapeDtypeStruct((block, features), half),
         in_specs=[pl.BlockSpec(memory_space=pl.ANY)] * len(operands),
         out_specs=pl.BlockSpec(memory_space=pltpu.VMEM),
@@ -496,16 +549,17 @@
             short((HALVES, cols, rows, POINTS, part, LANES), half),
             short((HALVES, cols, rows, part, features), half),
             short((POINTS, LANES, features), wide),
-            dma((steps,)),
+            short((width_in, LANES), wide),
+            dma((len(marks) - 1,)),
             dma((8,)),
             dma(()),
             dma((HALVES,)),
             dma((5,)),
             dma((HALVES,)),
-            dma((HALVES, rows // 2)),
+            dma((len(groups), rows // 2)),
             dma((HALVES,)),
-            dma((HALVES, rows // 2)),
-            dma((HALVES, 2)),
+            dma((len(groups),)),
+            dma((HALVES + len(groups),)),
         ],
         compiler_params=pltpu.CompilerParams(
             collective_id=0, has_side_effects=True, vmem_limit_bytes=32 * 1024 * 1024

time: 37.9 us -> 36.3 us (0.958)
  the two profiles are of different devices: /device:TPU:9 before, /device:TPU:1 now
where the time goes in v3:
time: 36.3 us; the launch traced here: 36.1 us
  Pallas kernels  35.1 us (97%)
  local copies, waits for them, and re-layouts  0.97 us (3%)
    pallas_call x1, Pallas kernels, fused(): pl.pallas_call(functools.partial(mixer_kernel, marks, 4, groups), out_sha...  35.1 us
    unnamed x1, local copies, waits for them, and re-layouts  0.97 us

profile of v3, /device:TPU:1, one launch (start us, length us, event | category | flops | bytes accessed | tf_op | source)
XLA Modules:
  0.0 36.1 jit_solution(675364214969917604)
XLA Ops:
  0.0 35.1 %shard_map.91 = bf16[1024,512]{1,0:T(8,128)(2,1)S(1)} custom-call(bf16[1024,2048]{1,0:T(8,128)(2,1)} %tokens_hbm.1, f32[1,2048]{1,0:T(1,128)} %bitcast.1, bf16[2048,256]{1,0:T(8,128)(2,1)} %w_in_hbm.1, bf16[1024,512]{1,0:T(8,128)(2,1)} %w_out_hbm.1, bf16[256,256]{1,0:T(8,128)(2,1)} %constant.10.clone.forward_hbm, bf16[256,256]{1,0:T(8,128)(2,1)} %constant.11.clone.fold_hbm, ...), custom_call_target="tpu_custom_call" | custom-call | tf_op jit(solution)/shard_map/pallas_call | solution.py:537
  35.2 1.0 %copy.11 = bf16[1024,512]{1,0:T(8,128)(2,1)} copy(bf16[1024,512]{1,0:T(8,128)(2,1)S(1)} %shard_map.91) | data formatting | bytes 2097152

commit v4 on v3

--- a/solution.py
+++ b/solution.py
@@ -496,6 +496,8 @@
     relay(1, inner)
     relay(2, outer)
     relay(2, inner)
+    relay(3, outer)
+    relay(3, inner)
     for g in range(1, len(groups)):
         share_far(g)
     pass_on(0)
@@ -533,7 +535,8 @@
     operands = [tokens, norm_gain[None, :], w_in, w_out, forward, fold, twiddles, coarse, fine]
     operands = [pltpu.with_memory_space_constraint(jnp.asarray(x), pltpu.HBM) for x in operands]
     dma = pltpu.SemaphoreType.DMA
-    groups = ((0, 0, POINTS), (1, 0, POINTS // 2), (1, POINTS // 2, POINTS // 2))
+    quad = POINTS // 4
+    groups = ((0, 0, POINTS), (1, 0, 2 * quad), (1, 2 * quad, quad), (1, 3 * quad, quad))
     return pl.pallas_call(
         functools.partial(mixer_kernel, marks, 4, groups),
         out_shape=jax.ShapeDtypeStruct((block, features), half),

time: 36.3 us -> 36.1 us (level)
  no operation moved by 1% of the time
where the time goes in v4:
time: 36.1 us; the launch traced here: 36 us
  Pallas kernels  35 us (97%)
  local copies, waits for them, and re-layouts  0.97 us (3%)
    pallas_call x1, Pallas kernels, fused(): pl.pallas_call(functools.partial(mixer_kernel, marks, 4, groups), out_sha...  35 us
    unnamed x1, local copies, waits for them, and re-layouts  0.97 us

profile of v4, /device:TPU:1, one launch (start us, length us, event | category | flops | bytes accessed | tf_op | source)
XLA Modules:
  0.0 36.0 jit_solution(3858310515363724550)
XLA Ops:
  0.0 35.0 %shard_map.91 = bf16[1024,512]{1,0:T(8,128)(2,1)S(1)} custom-call(bf16[1024,2048]{1,0:T(8,128)(2,1)} %tokens_hbm.1, f32[1,2048]{1,0:T(1,128)} %bitcast.1, bf16[2048,256]{1,0:T(8,128)(2,1)} %w_in_hbm.1, bf16[1024,512]{1,0:T(8,128)(2,1)} %w_out_hbm.1, bf16[256,256]{1,0:T(8,128)(2,1)} %constant.10.clone.forward_hbm, bf16[256,256]{1,0:T(8,128)(2,1)} %constant.11.clone.fold_hbm, ...), custom_call_target="tpu_custom_call" | custom-call | tf_op jit(solution)/shard_map/pallas_call | solution.py:540
  35.0 1.0 %copy.11 = bf16[1024,512]{1,0:T(8,128)(2,1)} copy(bf16[1024,512]{1,0:T(8,128)(2,1)S(1)} %shard_map.91) | data formatting | bytes 2097152

commit v5 on v4

--- a/solution.py
+++ b/solution.py
@@ -308,7 +308,7 @@
         for d in order:
             first_send(0, d, where).start()
     def second_half():
-        for d in order:
+        for d in [2, 3, 1] + far:
             first_send(1, d, pl.ds(0, block)).start()
 
     second_half()

time: 36.1 us -> 36.1 us (level)
  no operation moved by 1% of the time
where the time goes in v5:
time: 36.1 us; the launch traced here: 36 us
  Pallas kernels  35 us (97%)
  local copies, waits for them, and re-layouts  0.97 us (3%)
    pallas_call x1, Pallas kernels, fused(): pl.pallas_call(functools.partial(mixer_kernel, marks, 4, groups), out_sha...  35 us
    unnamed x1, local copies, waits for them, and re-layouts  0.97 us

profile of v5, /device:TPU:1, one launch (start us, length us, event | category | flops | bytes accessed | tf_op | source)
XLA Modules:
  0.0 36.0 jit_solution(12489383619720796383)
XLA Ops:
  0.0 35.0 %shard_map.91 = bf16[1024,512]{1,0:T(8,128)(2,1)S(1)} custom-call(bf16[1024,2048]{1,0:T(8,128)(2,1)} %tokens_hbm.1, f32[1,2048]{1,0:T(1,128)} %bitcast.1, bf16[2048,256]{1,0:T(8,128)(2,1)} %w_in_hbm.1, bf16[1024,512]{1,0:T(8,128)(2,1)} %w_out_hbm.1, bf16[256,256]{1,0:T(8,128)(2,1)} %constant.10.clone.forward_hbm, bf16[256,256]{1,0:T(8,128)(2,1)} %constant.11.clone.fold_hbm, ...), custom_call_target="tpu_custom_call" | custom-call | tf_op jit(solution)/shard_map/pallas_call | solution.py:540
  35.0 1.0 %copy.11 = bf16[1024,512]{1,0:T(8,128)(2,1)} copy(bf16[1024,512]{1,0:T(8,128)(2,1)S(1)} %shard_map.91) | data formatting | bytes 2097152
